TPU v7x, 256 devices: a 4x2x16 block of a 4x16x16 slice. The times are simulated.
256 devices in a mesh: grp: 2 (over y), fs: 16 (over z), tp: 8 (over x, core).
Axes of the slice: x: 4, y: 2, z: 16, core: 2. Of those that a mesh axis runs over, the one named last changes fastest.
The devices are a block of a 4x16x16 slice.
Arguments:
- tokens: bfloat16 [128, 128, 2048], P(('grp', 'fs'), None, 'tp'), parts along dimension 0, may hold values from -100 to 100
- mix_gain: float32 [2048], replicated, may hold values from 0.1 to 1.9
- gate_outer: bfloat16 [2048, 1024], P('fs', 'tp'), may hold values from -0.125 to 0.125
- gate_inner: bfloat16 [2048, 1024], P('fs', 'tp'), may hold values from -0.125 to 0.125
- value_weight: bfloat16 [2048, 1024], P('fs', 'tp'), may hold values from -0.125 to 0.125
- conv_taps: float32 [3, 1024], replicated, may hold values from -3 to 3
- mix_out: bfloat16 [1024, 2048], P('tp', 'fs'), may hold values from -0.25 to 0.25
- ffn_gain: float32 [2048], replicated, may hold values from 0.1 to 1.9
- ffn_gate: bfloat16 [2048, 5632], P('fs', 'tp'), may hold values from -0.125 to 0.125
- ffn_up: bfloat16 [2048, 5632], P('fs', 'tp'), may hold values from -0.125 to 0.125
- ffn_down: bfloat16 [5632, 2048], P('tp', 'fs'), may hold values from -0.109375 to 0.109375
- out_gain: float32 [2048], replicated, may hold values from 0.1 to 1.9
Outputs:
- layer_out: bfloat16 [128, 128, 2048], P(('grp', 'fs'), None, 'tp'), parts along dimension 0
There are 2 independent parts, one for each index of `grp`. A program takes and returns all parts, laid end to end along the dimension named above; an argument that names none is the same for every part. Nothing has to cross between parts.
All inputs are finite; a program needn't handle non-finite values.
Results may differ from a plain program's by a relative error of at most 0.015.
Values may be sent and summed in bfloat16 or wider, within the bound.
No kernel may reach another device: no remote copies, remote signals or barrier semaphores. Data moves between devices by JAX's collectives and lax.ppermute only.
A program may use at most 64 MiB of HBM per device.

v0:
```python
import jax
import jax.numpy as jnp
from jax import lax
from jax.sharding import PartitionSpec as P


def in_order(parts, dim):
    parts = jnp.moveaxis(parts, 0, dim)
    shape = parts.shape
    return parts.reshape(*shape[:dim], shape[dim] * shape[dim + 1], *shape[dim + 2 :])


def copy_for_each(shard, axis):
    copies = jnp.broadcast_to(shard, (lax.axis_size(axis), *shard.shape))
    return lax.all_to_all(copies, axis, split_axis=0, concat_axis=0, tiled=True)


def collect(shard, axis, dim):
    return in_order(copy_for_each(shard, axis), dim)


def side_by_side(arrays, axis, dim, along):
    both = jnp.concatenate(arrays, axis=along)
    filled, at, outs = (lax.all_gather(both, axis, axis=dim, tiled=True), 0, [])
    for a in arrays:
        outs.append(lax.slice_in_dim(filled, at, at + a.shape[along], axis=along))
        at += a.shape[along]
    return tuple(outs)


def in_blocks(shard, dim, count):
    shape = shard.shape
    parts = shard.reshape(*shape[:dim], count, shape[dim] // count, *shape[dim + 1 :])
    return jnp.moveaxis(parts, dim, 0)


def summed_on_arrival(shard, axis, dim):
    parts = in_blocks(shard, dim, lax.axis_size(axis))
    arrived = lax.all_to_all(parts, axis, split_axis=0, concat_axis=0, tiled=True)
    return arrived.astype(jnp.float32).sum(axis=0)


def of_everyone(shard, axis):
    return copy_for_each(shard, axis).sum(axis=0)


def rms_norm(values, gain):
    floats = values.astype(jnp.float32)
    scaled = floats * lax.rsqrt(jnp.mean(floats * floats, axis=-1, keepdims=True) + 1e-06)
    return (scaled * gain).astype(jnp.bfloat16)


def local(
    tokens,
    mix_gain,
    gate_outer,
    gate_inner,
    value_weight,
    conv_taps,
    mix_out,
    ffn_gain,
    ffn_gate,
    ffn_up,
    ffn_down,
    out_gain,
):
    seq_count, length, columns = tokens.shape
    row_count = seq_count * length
    width = columns * lax.axis_size("tp")
    whole = collect(tokens, "tp", 2).reshape(row_count, width)
    normed = rms_norm(whole, mix_gain)
    channels = gate_outer.shape[1]
    pieces = side_by_side((gate_outer, gate_inner, value_weight), "fs", 0, 1)
    sliced = normed
    outer = jnp.dot(sliced, pieces[0], preferred_element_type=jnp.float32)
    inner = jnp.dot(sliced, pieces[1], preferred_element_type=jnp.float32)
    values = jnp.dot(sliced, pieces[2], preferred_element_type=jnp.float32)
    outer = outer.astype(jnp.bfloat16)
    inner = inner.astype(jnp.bfloat16)
    values = values.astype(jnp.bfloat16)
    product = (inner.astype(jnp.float32) * values.astype(jnp.float32)).reshape(
        seq_count, length, channels
    )
    own_taps = lax.dynamic_slice_in_dim(conv_taps, lax.axis_index("tp") * channels, channels, 1)
    tap_count = conv_taps.shape[0]
    padded = jnp.pad(product, ((0, 0), (tap_count - 1, 0), (0, 0)))
    conv = jnp.zeros((seq_count, length, channels), jnp.float32)
    for offset in range(tap_count):
        conv = conv + own_taps[offset] * padded[:, offset : offset + length]
    gated = (outer.astype(jnp.float32) * conv.reshape(row_count, channels)).astype(jnp.bfloat16)
    mix_terms = jnp.dot(gated, collect(mix_out, "fs", 1), preferred_element_type=jnp.float32)
    mix_summed = summed_on_arrival(mix_terms.astype(jnp.bfloat16), "tp", 1)
    first = (tokens.reshape(row_count, columns).astype(jnp.float32) + mix_summed).astype(
        jnp.bfloat16
    )
    whole_ffn = collect(first.reshape(seq_count, length, columns), "tp", 2).reshape(
        row_count, width
    )
    normed_ffn = rms_norm(whole_ffn, ffn_gain)
    pieces = side_by_side((ffn_gate, ffn_up), "fs", 0, 1)
    sliced = normed_ffn
    gate = jnp.dot(sliced, pieces[0], preferred_element_type=jnp.float32)
    upward = jnp.dot(sliced, pieces[1], preferred_element_type=jnp.float32)
    hidden = (jax.nn.silu(gate) * upward).astype(jnp.bfloat16)
    down_terms = jnp.dot(
        hidden,
        lax.all_gather(ffn_down, "fs", axis=1, tiled=True),
        preferred_element_type=jnp.float32,
    )
    down_summed = summed_on_arrival(down_terms.astype(jnp.bfloat16), "tp", 1)
    second = first.astype(jnp.float32) + down_summed
    squares = of_everyone(jnp.sum(second * second, axis=1), "tp")
    factor = lax.rsqrt(squares / width + 1e-06)
    own_gain = lax.dynamic_slice_in_dim(out_gain, lax.axis_index("tp") * columns, columns, 0)
    result = second * factor[:, None] * own_gain
    return result.astype(jnp.bfloat16).reshape(seq_count, length, columns)


def solution(mesh):
    in_specs = (
        P(("grp", "fs"), None, "tp"),
        P(),
        P("fs", "tp"),
        P("fs", "tp"),
        P("fs", "tp"),
        P(),
        P("tp", "fs"),
        P(),
        P("fs", "tp"),
        P("fs", "tp"),
        P("tp", "fs"),
        P(),
    )
    out_specs = P(("grp", "fs"), None, "tp")
    return jax.shard_map(local, mesh=mesh, in_specs=in_specs, out_specs=out_specs, check_vma=False)
```

profile of v0, /device:TPU:33, one launch (start us, length us, event | category | flops | bytes accessed | tf_op | source)
XLA Modules:
  0.0 347.9 jit_solution(9210337294262374817)
XLA Ops:
  6.6 1.5 pad_maximum_fusion.1
  8.1 1.8 pad_maximum_fusion
  10.0 2.5 broadcast_in_dim.20
  12.5 24.1 %all-to-all-start = ((bf16[8,4,128,256]{3,2,1,0:T(8,128)(2,1)}), bf16[8,4,128,256]{3,2,1,0:T(8,128)(2,1)S(1)}, u32[]{:S(2)}, u32[]{:S(2)}) async-start(bf16[8,4,128,256]{3,2,1,0:T(8,128)(2,1)} %broadcast_in_dim.20), calls=%async_computation | async-start | bytes 4194304 | tf_op jit(solution)/shard_map/all_to_all | solution.py:15
  36.7 26.1 %all-to-all-done = bf16[8,4,128,256]{3,2,1,0:T(8,128)(2,1)S(1)} async-done(((bf16[8,4,128,256]{3,2,1,0:T(8,128)(2,1)}), bf16[8,4,128,256]{3,2,1,0:T(8,128)(2,1)S(1)}, u32[]{:S(2)}, u32[]{:S(2)}) %all-to-all-start) | async-done | bytes 2097184 | tf_op jit(solution)/shard_map/all_to_all | solution.py:15
  62.9 0.9 broadcast_in_dim.21
  63.7 5.7 %all-to-all-start.1 = ((bf16[16,128,128]{1,2,0:T(8,128)(2,1)}), bf16[16,128,128]{1,2,0:T(8,128)(2,1)S(1)}, u32[]{:S(2)}, u32[]{:S(2)}) async-start(bf16[16,128,128]{1,2,0:T(8,128)(2,1)} %broadcast_in_dim.21), calls=%async_computation.1 | async-start | bytes 1048576 | tf_op jit(solution)/shard_map/all_to_all | solution.py:15
  69.4 0.5 convert_bitcast_fusion.1
  70.0 2.4 copy.24
  72.4 2.0 copy.33
  75.5 23.0 %all-gather.4.cloned.1.call-done = bf16[2048,384]{1,0:T(8,128)(2,1)} async-done(((bf16[128,384]{1,0:T(8,128)(2,1)}), bf16[2048,384]{1,0:T(8,128)(2,1)}) %all-gather.4.cloned.1.call-update) | async-done | bytes 1572880 | tf_op jit(solution)/shard_map/all_gather | solution.py:24
  98.4 1.7 fusion.14
  100.2 1.8 fusion.13
  102.1 4.7 %convolution_convert_fusion = bf16[512,2048]{1,0:T(8,128)(2,1)} fusion(bf16[128,2048]{0,1:T(8,128)(2,1)S(1)} %bitcast.61, f32[512,128]{1,0:T(8,128)S(1)} %bitcast.63, bf16[512,2048]{1,0:T(8,128)(2,1)S(1)} %multiply_convert_fusion.1, bf16[2048,384]{1,0:T(8,128)(2,1)} %all-gather.4.cloned.1.call-done), kind=kOutput, calls=%fused_computation.10 | convolution fusion | flops 538181632 | bytes 5505024 | tf_op jit(solution)/shard_map/dot_general | solution.py:91
  106.7 3.1 copy.38
  109.8 13.0 %all-to-all-start.2 = ((bf16[8,512,256]{2,1,0:T(8,128)(2,1)}), bf16[8,512,256]{2,1,0:T(8,128)(2,1)S(1)}, u32[]{:S(2)}, u32[]{:S(2)}) async-start(bf16[8,512,256]{2,1,0:T(8,128)(2,1)} %bitcast.53), calls=%async_computation.2 | async-start | bytes 4194304 | tf_op jit(solution)/shard_map/all_to_all | solution.py:39
  122.9 0.7 all-gather.8.cloned.1.call-update
  123.6 25.4 %all-to-all-done.2 = bf16[8,512,256]{2,1,0:T(8,128)(2,1)S(1)} async-done(((bf16[8,512,256]{2,1,0:T(8,128)(2,1)}), bf16[8,512,256]{2,1,0:T(8,128)(2,1)S(1)}, u32[]{:S(2)}, u32[]{:S(2)}) %all-to-all-start.2) | async-done | bytes 2097184 | tf_op jit(solution)/shard_map/all_to_all | solution.py:39
  149.7 29.7 %all_to_all.31 = bf16[8,4,128,256]{3,2,1,0:T(8,128)(2,1)S(1)} all-to-all(bf16[8,4,128,256]{3,2,1,0:T(8,128)(2,1)S(1)} %broadcast_in_dim.22), channel_id=1, replica_groups=mesh['grp'=2,'fs'=16,'tp'=8] {'tp'}, dimensions={0} | all-to-all | bytes 4194304 | tf_op jit(solution)/shard_map/all_to_all | solution.py:15
  179.4 0.5 convert_bitcast_fusion
  179.9 2.4 copy.27
  182.3 4.0 %copy.34 = f32[64,8,8,256]{3,1,2,0:T(8,128)} copy(f32[64,8,8,256]{3,2,1,0:T(8,128)S(1)} %bitcast.52) | data formatting | bytes 8388608
  186.8 13.6 %all-gather.6.cloned.1.call-done = bf16[2048,1408]{0,1:T(8,128)(2,1)} async-done(((bf16[128,1408]{0,1:T(8,128)(2,1)}), bf16[2048,1408]{0,1:T(8,128)(2,1)}) %all-gather.6.cloned.1.call-update) | async-done | bytes 5767184 | tf_op jit(solution)/shard_map/all_gather | solution.py:24
  200.4 6.0 %fusion.4 = f32[512,704]{0,1:T(8,128)} fusion(bf16[2048,1408]{0,1:T(8,128)(2,1)} %all-gather.6.cloned.1.call-done, f32[512,2048]{1,0:T(8,128)} %bitcast.57, f32[2048]{0:T(1024)S(1)} %copy-done.4, f32[512]{0:T(512)S(1)} %rsqrt_bitcast_fusion.1), kind=kOutput, calls=%fused_computation.14 | convolution fusion | flops 1479540736 | bytes 8529920 | tf_op jit(solution)/shard_map/dot_general | solution.py:102
  206.4 74.6 %all-gather.8.cloned.1.call-done = bf16[704,2048]{1,0:T(8,128)(2,1)} async-done(((bf16[704,128]{1,0:T(8,128)(2,1)}), bf16[704,2048]{1,0:T(8,128)(2,1)}) %all-gather.8.cloned.1.call-update) | async-done | bytes 2883600 | tf_op jit(solution)/shard_map/all_gather | solution.py:107
  281.0 7.8 %convolution_convert_fusion.1 = bf16[512,2048]{1,0:T(8,128)(2,1)S(1)} fusion(bf16[704,2048]{1,0:T(8,128)(2,1)} %all-gather.8.cloned.1.call-done, bf16[2048,1408]{0,1:T(8,128)(2,1)} %all-gather.6.cloned.1.call-done, f32[512,704]{0,1:T(8,128)} %fusion.4, f32[512,2048]{1,0:T(8,128)} %bitcast.58, f32[2048]{0:T(1024)S(1)} %copy-done.4, ...), kind=kOutput, calls=%fused_computation.11 | convolution fusion | flops 2959147008 | bytes 13510656 | tf_op jit(solution)/shard_map/dot_general | solution.py:105
  289.0 41.4 %all_to_all.32 = bf16[8,512,256]{2,1,0:T(8,128)(2,1)S(1)} all-to-all(bf16[8,512,256]{2,1,0:T(8,128)(2,1)S(1)} %bitcast.55), channel_id=1, replica_groups=mesh['grp'=2,'fs'=16,'tp'=8] {'tp'}, dimensions={0} | all-to-all | bytes 4194304 | tf_op jit(solution)/shard_map/all_to_all | solution.py:39
  330.9 0.6 broadcast_in_dim.24
  331.5 4.3 %all-to-all-start.5 = ((f32[8,1,512]{2,1,0:T(1,128)}), f32[8,1,512]{2,1,0:T(1,128)S(1)}, u32[]{:S(2)}, u32[]{:S(2)}) async-start(f32[8,1,512]{2,1,0:T(1,128)} %broadcast_in_dim.24), calls=%async_computation.5 | async-start | bytes 32768 | tf_op jit(solution)/shard_map/all_to_all | solution.py:15
  335.8 0.8 dynamic_slice.7
  336.6 4.0 %all-to-all-done.5 = f32[8,1,512]{2,1,0:T(1,128)S(1)} async-done(((f32[8,1,512]{2,1,0:T(1,128)}), f32[8,1,512]{2,1,0:T(1,128)S(1)}, u32[]{:S(2)}, u32[]{:S(2)}) %all-to-all-start.5) | async-done | bytes 16416 | tf_op jit(solution)/shard_map/all_to_all | solution.py:15
  340.6 0.8 multiply_convert_fusion.2
  (33 shorter events, 3.2 us)
Async XLA Ops:
  6.5 30.1 %copy-start = (f32[3,1024]{1,0:T(4,128)S(1)}, f32[3,1024]{1,0:T(4,128)}, u32[]{:S(2)}) copy-start(f32[3,1024]{1,0:T(4,128)} %param.17) | copy-start | bytes 36868
  6.6 91.9 %all-gather.4.cloned.1.call-start = ((), (), s32[]{:S(2)}) async-start(), calls=%async_computation.6 | async-start | bytes 1671168 | tf_op jit(solution)/shard_map/all_gather | solution.py:24
  8.1 192.4 %all-gather.6.cloned.1.call-start = ((), (), s32[]{:S(2)}) async-start(), calls=%async_computation.7 | async-start | bytes 6127616 | tf_op jit(solution)/shard_map/all_gather | solution.py:24
  12.5 24.1 %copy-start.2 = (bf16[128,128]{1,0:T(8,128)(2,1)S(1)}, bf16[128,128]{1,0:T(8,128)(2,1)}, u32[]{:S(2)}) copy-start(bf16[128,128]{1,0:T(8,128)(2,1)} %param.18) | copy-start | bytes 98308
  12.5 50.4 %all-to-all-start = ((bf16[8,4,128,256]{3,2,1,0:T(8,128)(2,1)}), bf16[8,4,128,256]{3,2,1,0:T(8,128)(2,1)S(1)}, u32[]{:S(2)}, u32[]{:S(2)}) async-start(bf16[8,4,128,256]{3,2,1,0:T(8,128)(2,1)} %broadcast_in_dim.20), calls=%async_computation | async-start | bytes 4194304 | tf_op jit(solution)/shard_map/all_to_all | solution.py:15
  63.7 38.3 %all-to-all-start.1 = ((bf16[16,128,128]{1,2,0:T(8,128)(2,1)}), bf16[16,128,128]{1,2,0:T(8,128)(2,1)S(1)}, u32[]{:S(2)}, u32[]{:S(2)}) async-start(bf16[16,128,128]{1,2,0:T(8,128)(2,1)} %broadcast_in_dim.21), calls=%async_computation.1 | async-start | bytes 1048576 | tf_op jit(solution)/shard_map/all_to_all | solution.py:15
  74.4 0.7 copy-start.3
  109.8 39.2 %all-to-all-start.2 = ((bf16[8,512,256]{2,1,0:T(8,128)(2,1)}), bf16[8,512,256]{2,1,0:T(8,128)(2,1)S(1)}, u32[]{:S(2)}, u32[]{:S(2)}) async-start(bf16[8,512,256]{2,1,0:T(8,128)(2,1)} %bitcast.53), calls=%async_computation.2 | async-start | bytes 4194304 | tf_op jit(solution)/shard_map/all_to_all | solution.py:39
  122.9 26.5 %copy-start.1 = (bf16[4,128,256]{2,1,0:T(8,128)(2,1)S(1)}, bf16[4,128,256]{2,1,0:T(8,128)(2,1)}, u32[]{:S(2)}) copy-start(bf16[4,128,256]{2,1,0:T(8,128)(2,1)} %param.12) | copy-start | bytes 786436
  122.9 158.1 %all-gather.8.cloned.1.call-start = ((), (), s32[]{:S(2)}) async-start(), calls=%async_computation.8 | async-start | bytes 3063808 | tf_op jit(solution)/shard_map/all_gather | solution.py:107
  186.3 14.1 %copy-start.4 = (f32[2048]{0:T(1024)S(1)}, f32[2048]{0:T(1024)}, u32[]{:S(2)}) copy-start(f32[2048]{0:T(1024)} %param.19) | copy-start | bytes 24580
  331.5 9.0 %all-to-all-start.5 = ((f32[8,1,512]{2,1,0:T(1,128)}), f32[8,1,512]{2,1,0:T(1,128)S(1)}, u32[]{:S(2)}, u32[]{:S(2)}) async-start(f32[8,1,512]{2,1,0:T(1,128)} %broadcast_in_dim.24), calls=%async_computation.5 | async-start | bytes 32768 | tf_op jit(solution)/shard_map/all_to_all | solution.py:15
Sparse Core Ops, SparseCore 0:
  9.1 89.2 all-gather.3
  100.2 100.1 all-gather.5
  202.2 78.7 all-gather.7
where the time goes:
time: 349 us; the launch traced here: 348 us
  waiting for transfers between devices  168 us (48%)
  blocking collectives  71.1 us (20%)
  starting transfers between devices  47.1 us (13%)
  matrix products  22 us (6%)
  local copies, waits for them, and re-layouts  19.4 us (6%)
  between operations  13.3 us (4%)
  other arithmetic  7.44 us (2%)
    all_gather x1, waiting for transfers between devices, local(): lax.all_gather(ffn_down, 'fs', axis=1, tiled=True)  74.6 us
    all_to_all x1, blocking collectives, summed_on_arrival(): lax.all_to_all(parts, axis, split_axis=0, concat_axis=0, tiled=True)  41.4 us
    all_gather x2, waiting for transfers between devices, side_by_side(): filled, at, outs = (lax.all_gather(both, axis, axis=dim, tiled=True), 0, [])  36.6 us
    all_to_all x3, starting transfers between devices, copy_for_each(): return lax.all_to_all(copies, axis, split_axis=0, concat_axis=0, tiled=True)  34 us
    all_to_all x3, waiting for transfers between devices, copy_for_each(): return lax.all_to_all(copies, axis, split_axis=0, concat_axis=0, tiled=True)  30.1 us
    all_to_all x1, blocking collectives, copy_for_each(): return lax.all_to_all(copies, axis, split_axis=0, concat_axis=0, tiled=True)  29.7 us
    all_to_all x1, waiting for transfers between devices, summed_on_arrival(): lax.all_to_all(parts, axis, split_axis=0, concat_axis=0, tiled=True)  25.4 us
    all_to_all x1, starting transfers between devices, summed_on_arrival(): lax.all_to_all(parts, axis, split_axis=0, concat_axis=0, tiled=True)  13 us
  transfers between devices with their start and end apart: 7, of which 6 were waited for; matrix products, arithmetic and copies ran while one was open for 11% of the time, Pallas kernels for 0%

commit v1 on v0

--- a/solution.py
+++ b/solution.py
@@ -2,6 +2,27 @@
 import jax.numpy as jnp
 from jax import lax
 from jax.sharding import PartitionSpec as P
+
+
+def collect_2(x, axis, dim):
+    size, index, rows = (lax.axis_size(axis), lax.axis_index(axis), x.shape[dim])
+    right = [(i, (i + 1) % size) for i in range(size)]
+    left = [(i, (i - 1) % size) for i in range(size)]
+    whole = jnp.zeros((*x.shape[:dim], size * rows, *x.shape[dim + 1 :]), x.dtype)
+    whole = lax.dynamic_update_slice_in_dim(whole, x, index * rows, axis=dim)
+    from_left = from_right = x
+    half = size // 2
+    for lap in range(1, half + 1):
+        from_left = lax.ppermute(from_left, axis, right)
+        whole = lax.dynamic_update_slice_in_dim(
+            whole, from_left, (index - lap) % size * rows, axis=dim
+        )
+        if lap < size - half:
+            from_right = lax.ppermute(from_right, axis, left)
+            whole = lax.dynamic_update_slice_in_dim(
+                whole, from_right, (index + lap) % size * rows, axis=dim
+            )
+    return whole
 
 
 def in_order(parts, dim):
@@ -102,11 +123,7 @@
     gate = jnp.dot(sliced, pieces[0], preferred_element_type=jnp.float32)
     upward = jnp.dot(sliced, pieces[1], preferred_element_type=jnp.float32)
     hidden = (jax.nn.silu(gate) * upward).astype(jnp.bfloat16)
-    down_terms = jnp.dot(
-        hidden,
-        lax.all_gather(ffn_down, "fs", axis=1, tiled=True),
-        preferred_element_type=jnp.float32,
-    )
+    down_terms = jnp.dot(hidden, collect_2(ffn_down, "fs", 1), preferred_element_type=jnp.float32)
     down_summed = summed_on_arrival(down_terms.astype(jnp.bfloat16), "tp", 1)
     second = first.astype(jnp.float32) + down_summed
     squares = of_everyone(jnp.sum(second * second, axis=1), "tp")

time: 349 us -> 299 us (0.86)
  waiting for transfers between devices: 168 us -> 114 us
  blocking collectives: 71.1 us -> 39.2 us
  starting transfers between devices: 47.1 us -> 68.2 us
  local copies, waits for them, and re-layouts: 19.4 us -> 33.9 us
    all_gather x1 -> x0, waiting for transfers between devices: 74.6 us -> none  [local(): lax.all_gather(ffn_down, 'fs', axis=1, tiled=True)]
    ppermute x0 -> x15, waiting for transfers between devices: none -> 37.4 us  [the longest x8 25.4 us: collect_2(): from_left = lax.ppermute(from_left, axis, right)]
    all_to_all x1 -> x0, blocking collectives: 29.7 us -> none  [copy_for_each(): return lax.all_to_all(copies, axis, split_axis=0, concat_axis=0, tiled=True)]
    ppermute x0 -> x15, starting transfers between devices: none -> 16.2 us  [the longest x7 11 us: collect_2(): from_right = lax.ppermute(from_right, axis, left)]
    all_gather x2, waiting for transfers between devices: 36.6 us -> 23 us  [side_by_side(): filled, at, outs = (lax.all_gather(both, axis, axis=dim, tiled=True), 0, [])]
    dynamic_update_slice x0 -> x16, local copies, waits for them, and re-layouts: none -> 11.3 us  [the longest x8 5.68 us: collect_2(): lax.dynamic_update_slice_in_dim(whole, from_left, (index - lap) % size *...]
    all_to_all x3 -> x4, starting transfers between devices: 34 us -> 38.4 us  [copy_for_each(): return lax.all_to_all(copies, axis, split_axis=0, concat_axis=0, tiled=True)]
    all_to_all x3 -> x4, waiting for transfers between devices: 30.1 us -> 30.1 us  [copy_for_each(): return lax.all_to_all(copies, axis, split_axis=0, concat_axis=0, tiled=True)]
  transfers between devices with their start and end apart: 7 -> 22, of which waited for: 6 -> 16; matrix products, arithmetic and copies ran while one was open for 11% -> 15% of each run, Pallas kernels for 0% -> 0%
where the time goes in v1:
time: 299 us; the launch traced here: 298 us
  waiting for transfers between devices  114 us (38%)
  starting transfers between devices  68.2 us (23%)
  blocking collectives  39.2 us (13%)
  local copies, waits for them, and re-layouts  33.9 us (11%)
  matrix products  22 us (7%)
  between operations  13.7 us (5%)
  other arithmetic  7.43 us (2%)
    all_to_all x1, blocking collectives, summed_on_arrival(): lax.all_to_all(parts, axis, split_axis=0, concat_axis=0, tiled=True)  39.2 us
    all_to_all x4, starting transfers between devices, copy_for_each(): return lax.all_to_all(copies, axis, split_axis=0, concat_axis=0, tiled=True)  38.4 us
    all_to_all x4, waiting for transfers between devices, copy_for_each(): return lax.all_to_all(copies, axis, split_axis=0, concat_axis=0, tiled=True)  30.1 us
    ppermute x8, waiting for transfers between devices, collect_2(): from_left = lax.ppermute(from_left, axis, right)  25.4 us
    all_to_all x1, waiting for transfers between devices, summed_on_arrival(): lax.all_to_all(parts, axis, split_axis=0, concat_axis=0, tiled=True)  23.5 us
    all_gather x2, waiting for transfers between devices, side_by_side(): filled, at, outs = (lax.all_gather(both, axis, axis=dim, tiled=True), 0, [])  23 us
    all_to_all x1, starting transfers between devices, summed_on_arrival(): lax.all_to_all(parts, axis, split_axis=0, concat_axis=0, tiled=True)  13.6 us
    ppermute x7, waiting for transfers between devices, collect_2(): from_right = lax.ppermute(from_right, axis, left)  12 us
  transfers between devices with their start and end apart: 22, of which 16 were waited for; matrix products, arithmetic and copies ran while one was open for 15% of the time, Pallas kernels for 0%

profile of v1, /device:TPU:33, one launch (start us, length us, event | category | flops | bytes accessed | tf_op | source)
XLA Modules:
  0.0 298.4 jit_solution(6325165433068159113)
XLA Ops:
  10.0 2.5 broadcast_in_dim.23
  12.5 23.9 %all-to-all-start = ((bf16[8,4,128,256]{3,2,1,0:T(8,128)(2,1)}), bf16[8,4,128,256]{3,2,1,0:T(8,128)(2,1)S(1)}, u32[]{:S(2)}, u32[]{:S(2)}) async-start(bf16[8,4,128,256]{3,2,1,0:T(8,128)(2,1)} %broadcast_in_dim.23), calls=%async_computation | async-start | bytes 4194304 | tf_op jit(solution)/shard_map/all_to_all | solution.py:36
  36.6 26.1 %all-to-all-done = bf16[8,4,128,256]{3,2,1,0:T(8,128)(2,1)S(1)} async-done(((bf16[8,4,128,256]{3,2,1,0:T(8,128)(2,1)}), bf16[8,4,128,256]{3,2,1,0:T(8,128)(2,1)S(1)}, u32[]{:S(2)}, u32[]{:S(2)}) %all-to-all-start) | async-done | bytes 2097184 | tf_op jit(solution)/shard_map/all_to_all | solution.py:36
  63.7 5.7 %all-to-all-start.1 = ((bf16[16,128,128]{1,2,0:T(8,128)(2,1)}), bf16[16,128,128]{1,2,0:T(8,128)(2,1)S(1)}, u32[]{:S(2)}, u32[]{:S(2)}) async-start(bf16[16,128,128]{1,2,0:T(8,128)(2,1)} %broadcast_in_dim.24), calls=%async_computation.1 | async-start | bytes 1048576 | tf_op jit(solution)/shard_map/all_to_all | solution.py:36
  69.9 2.4 copy.24
  75.2 23.0 %all-gather.3.cloned.1.call-done = bf16[2048,384]{1,0:T(8,128)(2,1)} async-done(((bf16[128,384]{1,0:T(8,128)(2,1)}), bf16[2048,384]{1,0:T(8,128)(2,1)}) %all-gather.3.cloned.1.call-update) | async-done | bytes 1572880 | tf_op jit(solution)/shard_map/all_gather | solution.py:45
  101.8 4.7 %convolution_convert_fusion = bf16[512,2048]{1,0:T(8,128)(2,1)} fusion(bf16[128,2048]{0,1:T(8,128)(2,1)S(1)} %bitcast.61, f32[512,128]{1,0:T(8,128)S(1)} %bitcast.63, bf16[512,2048]{1,0:T(8,128)(2,1)S(1)} %multiply_convert_fusion.1, bf16[2048,384]{1,0:T(8,128)(2,1)} %all-gather.3.cloned.1.call-done), kind=kOutput, calls=%fused_computation.10 | convolution fusion | flops 538181632 | bytes 5505024 | tf_op jit(solution)/shard_map/dot_general | solution.py:112
  106.4 3.1 %copy.38 = bf16[64,8,8,256]{3,2,0,1:T(8,128)(2,1)} copy(bf16[64,8,8,256]{3,2,1,0:T(8,128)(2,1)} %bitcast.54) | data formatting | bytes 4194304 | tf_op jit(solution)/shard_map/reshape | solution.py:54
  109.6 13.6 %all-to-all-start.2 = ((bf16[8,512,256]{2,1,0:T(8,128)(2,1)}), bf16[8,512,256]{2,1,0:T(8,128)(2,1)S(1)}, u32[]{:S(2)}, u32[]{:S(2)}) async-start(bf16[8,512,256]{2,1,0:T(8,128)(2,1)} %bitcast.53), calls=%async_computation.2 | async-start | bytes 4194304 | tf_op jit(solution)/shard_map/all_to_all | solution.py:60
  123.4 2.5 collective-permute-start.1
  125.8 23.5 %all-to-all-done.2 = bf16[8,512,256]{2,1,0:T(8,128)(2,1)S(1)} async-done(((bf16[8,512,256]{2,1,0:T(8,128)(2,1)}), bf16[8,512,256]{2,1,0:T(8,128)(2,1)S(1)}, u32[]{:S(2)}, u32[]{:S(2)}) %all-to-all-start.2) | async-done | bytes 2097184 | tf_op jit(solution)/shard_map/all_to_all | solution.py:60
  151.3 4.5 %all-to-all-start.3 = ((bf16[8,4,128,256]{3,2,1,0:T(8,128)(2,1)}), bf16[8,4,128,256]{3,2,1,0:T(8,128)(2,1)S(1)}, u32[]{:S(2)}, u32[]{:S(2)}) async-start(bf16[8,4,128,256]{3,2,1,0:T(8,128)(2,1)} %broadcast_in_dim.25), calls=%async_computation.3 | async-start | bytes 4194304 | tf_op jit(solution)/shard_map/all_to_all | solution.py:36
  155.8 2.0 broadcast_in_dim.26
  158.7 2.4 collective-permute-start.3
  162.5 6.3 %collective-permute-done.2 = bf16[704,128]{1,0:T(8,128)(2,1)S(1)} collective-permute-done((bf16[704,128]{1,0:T(8,128)(2,1)S(1)}, bf16[704,128]{1,0:T(8,128)(2,1)S(1)}, u32[]{:S(2)}, u32[]{:S(2)}) %collective-permute-start.2) | collective-permute-done | bytes 180256 | tf_op jit(solution)/shard_map/ppermute | solution.py:16
  168.8 2.7 collective-permute-start.5
  172.9 2.6 collective-permute-done.4
  175.5 2.3 collective-permute-start.6
  181.3 2.7 collective-permute-done.6
  185.5 2.2 collective-permute-done.7
  189.2 2.3 collective-permute-done.8
  192.4 4.7 %collective-permute-done.9 = bf16[704,128]{1,0:T(8,128)(2,1)S(1)} collective-permute-done((bf16[704,128]{1,0:T(8,128)(2,1)S(1)}, bf16[704,128]{1,0:T(8,128)(2,1)S(1)}, u32[]{:S(2)}, u32[]{:S(2)}) %collective-permute-start.9) | collective-permute-done | bytes 180256 | tf_op jit(solution)/shard_map/ppermute | solution.py:21
  200.6 3.7 %collective-permute-done.11 = bf16[704,128]{1,0:T(8,128)(2,1)S(1)} collective-permute-done((bf16[704,128]{1,0:T(8,128)(2,1)S(1)}, bf16[704,128]{1,0:T(8,128)(2,1)S(1)}, u32[]{:S(2)}, u32[]{:S(2)}) %collective-permute-start.11) | collective-permute-done | bytes 180256 | tf_op jit(solution)/shard_map/ppermute | solution.py:21
  207.4 3.1 %collective-permute-done.12 = bf16[704,128]{1,0:T(8,128)(2,1)S(1)} collective-permute-done((bf16[704,128]{1,0:T(8,128)(2,1)S(1)}, bf16[704,128]{1,0:T(8,128)(2,1)S(1)}, u32[]{:S(2)}, u32[]{:S(2)}) %collective-permute-start.12) | collective-permute-done | bytes 180256 | tf_op jit(solution)/shard_map/ppermute | solution.py:16
  212.8 6.5 %collective-permute-done.14 = bf16[704,128]{1,0:T(8,128)(2,1)S(1)} collective-permute-done((bf16[704,128]{1,0:T(8,128)(2,1)S(1)}, bf16[704,128]{1,0:T(8,128)(2,1)S(1)}, u32[]{:S(2)}, u32[]{:S(2)}) %collective-permute-start.14) | collective-permute-done | bytes 180256 | tf_op jit(solution)/shard_map/ppermute | solution.py:16
  220.5 2.4 copy.27
  223.0 4.0 %copy.34 = f32[64,8,8,256]{3,1,2,0:T(8,128)} copy(f32[64,8,8,256]{3,2,1,0:T(8,128)S(1)} %bitcast.52) | data formatting | bytes 8388608
  227.5 6.0 %fusion.4 = f32[512,704]{0,1:T(8,128)} fusion(bf16[2048,1408]{0,1:T(8,128)(2,1)} %all-gather.5.cloned.1.call-done, f32[512,2048]{1,0:T(8,128)} %bitcast.57, f32[2048]{0:T(1024)S(1)} %copy-done.6, f32[512]{0:T(512)S(1)} %rsqrt_bitcast_fusion.1), kind=kOutput, calls=%fused_computation.14 | convolution fusion | flops 1479540736 | bytes 8529920 | tf_op jit(solution)/shard_map/dot_general | solution.py:123
  233.5 7.8 %convolution_convert_fusion.1 = bf16[512,2048]{1,0:T(8,128)(2,1)S(1)} fusion(bf16[704,2048]{1,0:T(8,128)(2,1)} %constant_dynamic-update-slice_fusion, bf16[2048,1408]{0,1:T(8,128)(2,1)} %all-gather.5.cloned.1.call-done, f32[512,704]{0,1:T(8,128)} %fusion.4, f32[512,2048]{1,0:T(8,128)} %bitcast.58, f32[2048]{0:T(1024)S(1)} %copy-done.6, ...), kind=kOutput, calls=%fused_computation.11 | convolution fusion | flops 2959147008 | bytes 13510656 | tf_op jit(solution)/shard_map/dot_general | solution.py:126
  241.5 39.2 %all_to_all.31 = bf16[8,512,256]{2,1,0:T(8,128)(2,1)S(1)} all-to-all(bf16[8,512,256]{2,1,0:T(8,128)(2,1)S(1)} %bitcast.55), channel_id=1, replica_groups=mesh['grp'=2,'fs'=16,'tp'=8] {'tp'}, dimensions={0} | all-to-all | bytes 4194304 | tf_op jit(solution)/shard_map/all_to_all | solution.py:60
  281.7 4.3 %all-to-all-start.5 = ((f32[8,1,512]{2,1,0:T(1,128)}), f32[8,1,512]{2,1,0:T(1,128)S(1)}, u32[]{:S(2)}, u32[]{:S(2)}) async-start(f32[8,1,512]{2,1,0:T(1,128)} %broadcast_in_dim.28), calls=%async_computation.5 | async-start | bytes 32768 | tf_op jit(solution)/shard_map/all_to_all | solution.py:36
  286.8 4.0 %all-to-all-done.5 = f32[8,1,512]{2,1,0:T(1,128)S(1)} async-done(((f32[8,1,512]{2,1,0:T(1,128)}), f32[8,1,512]{2,1,0:T(1,128)S(1)}, u32[]{:S(2)}, u32[]{:S(2)}) %all-to-all-start.5) | async-done | bytes 16416 | tf_op jit(solution)/shard_map/all_to_all | solution.py:36
  (82 shorter events, 38.1 us)
Async XLA Ops:
  6.5 30.0 %copy-start = (f32[3,1024]{1,0:T(4,128)S(1)}, f32[3,1024]{1,0:T(4,128)}, u32[]{:S(2)}) copy-start(f32[3,1024]{1,0:T(4,128)} %param.17) | copy-start | bytes 36868
  6.6 91.6 %all-gather.3.cloned.1.call-start = ((), (), s32[]{:S(2)}) async-start(), calls=%async_computation.6 | async-start | bytes 1671168 | tf_op jit(solution)/shard_map/all_gather | solution.py:45
  8.1 219.4 %all-gather.5.cloned.1.call-start = ((), (), s32[]{:S(2)}) async-start(), calls=%async_computation.7 | async-start | bytes 6127616 | tf_op jit(solution)/shard_map/all_gather | solution.py:45
  10.0 26.5 %copy-start.4 = (bf16[128,128]{1,0:T(8,128)(2,1)S(1)}, bf16[128,128]{1,0:T(8,128)(2,1)}, u32[]{:S(2)}) copy-start(bf16[128,128]{1,0:T(8,128)(2,1)} %param.18) | copy-start | bytes 98308
  12.5 50.2 %all-to-all-start = ((bf16[8,4,128,256]{3,2,1,0:T(8,128)(2,1)}), bf16[8,4,128,256]{3,2,1,0:T(8,128)(2,1)S(1)}, u32[]{:S(2)}, u32[]{:S(2)}) async-start(bf16[8,4,128,256]{3,2,1,0:T(8,128)(2,1)} %broadcast_in_dim.23), calls=%async_computation | async-start | bytes 4194304 | tf_op jit(solution)/shard_map/all_to_all | solution.py:36
  63.7 38.1 %all-to-all-start.1 = ((bf16[16,128,128]{1,2,0:T(8,128)(2,1)}), bf16[16,128,128]{1,2,0:T(8,128)(2,1)S(1)}, u32[]{:S(2)}, u32[]{:S(2)}) async-start(bf16[16,128,128]{1,2,0:T(8,128)(2,1)} %broadcast_in_dim.24), calls=%async_computation.1 | async-start | bytes 1048576 | tf_op jit(solution)/shard_map/all_to_all | solution.py:36
  72.3 2.5 copy-start.5
  109.6 13.6 %copy-start.3 = (bf16[704,128]{1,0:T(8,128)(2,1)S(1)}, bf16[704,128]{1,0:T(8,128)(2,1)}, u32[]{:S(2)}) copy-start(bf16[704,128]{1,0:T(8,128)(2,1)} %param.22) | copy-start | bytes 540676
  109.6 40.1 %copy-start.2 = (bf16[4,128,256]{2,1,0:T(8,128)(2,1)S(1)}, bf16[4,128,256]{2,1,0:T(8,128)(2,1)}, u32[]{:S(2)}) copy-start(bf16[4,128,256]{2,1,0:T(8,128)(2,1)} %param.12) | copy-start | bytes 786436
  109.6 39.8 %all-to-all-start.2 = ((bf16[8,512,256]{2,1,0:T(8,128)(2,1)}), bf16[8,512,256]{2,1,0:T(8,128)(2,1)S(1)}, u32[]{:S(2)}, u32[]{:S(2)}) async-start(bf16[8,512,256]{2,1,0:T(8,128)(2,1)} %bitcast.53), calls=%async_computation.2 | async-start | bytes 4194304 | tf_op jit(solution)/shard_map/all_to_all | solution.py:60
  123.1 35.3 %collective-permute-start = (bf16[704,128]{1,0:T(8,128)(2,1)S(1)}, bf16[704,128]{1,0:T(8,128)(2,1)S(1)}, u32[]{:S(2)}, u32[]{:S(2)}) collective-permute-start(bf16[704,128]{1,0:T(8,128)(2,1)S(1)} %copy-done.3), channel_id=1, source_target_pairs={{0,8},{8,16},{16,24},{24,32},{32,40},{40,48},{48,56},{56,64},{64,7... | collective-permute-start | bytes 540680 | tf_op jit(solution)/shard_map/ppermute | solution.py:16
  123.4 35.3 %collective-permute-start.1 = (bf16[704,128]{1,0:T(8,128)(2,1)S(1)}, bf16[704,128]{1,0:T(8,128)(2,1)S(1)}, u32[]{:S(2)}, u32[]{:S(2)}) collective-permute-start(bf16[704,128]{1,0:T(8,128)(2,1)S(1)} %copy-done.3), channel_id=1, source_target_pairs={{0,120},{8,0},{16,8},{24,16},{32,24},{40,32},{48,40},{56,48},{64,5... | collective-permute-start | bytes 540680 | tf_op jit(solution)/shard_map/ppermute | solution.py:21
  151.3 68.7 %all-to-all-start.3 = ((bf16[8,4,128,256]{3,2,1,0:T(8,128)(2,1)}), bf16[8,4,128,256]{3,2,1,0:T(8,128)(2,1)S(1)}, u32[]{:S(2)}, u32[]{:S(2)}) async-start(bf16[8,4,128,256]{3,2,1,0:T(8,128)(2,1)} %broadcast_in_dim.25), calls=%async_computation.3 | async-start | bytes 4194304 | tf_op jit(solution)/shard_map/all_to_all | solution.py:36
  158.4 10.4 %collective-permute-start.2 = (bf16[704,128]{1,0:T(8,128)(2,1)S(1)}, bf16[704,128]{1,0:T(8,128)(2,1)S(1)}, u32[]{:S(2)}, u32[]{:S(2)}) collective-permute-start(bf16[704,128]{1,0:T(8,128)(2,1)S(1)} %collective-permute-done), channel_id=1, source_target_pairs={{0,8},{8,16},{16,24},{24,32},{32,40},{40,48},{48,56},{56,64},{64,7... | collective-permute-start | bytes 540680 | tf_op jit(solution)/shard_map/ppermute | solution.py:16
  158.7 10.2 %collective-permute-start.3 = (bf16[704,128]{1,0:T(8,128)(2,1)S(1)}, bf16[704,128]{1,0:T(8,128)(2,1)S(1)}, u32[]{:S(2)}, u32[]{:S(2)}) collective-permute-start(bf16[704,128]{1,0:T(8,128)(2,1)S(1)} %collective-permute-done.1), channel_id=1, source_target_pairs={{0,120},{8,0},{16,8},{24,16},{32,24},{40,32},{48,40},{56,48},{64,5... | collective-permute-start | bytes 540680 | tf_op jit(solution)/shard_map/ppermute | solution.py:21
  168.8 6.6 %collective-permute-start.4 = (bf16[704,128]{1,0:T(8,128)(2,1)S(1)}, bf16[704,128]{1,0:T(8,128)(2,1)S(1)}, u32[]{:S(2)}, u32[]{:S(2)}) collective-permute-start(bf16[704,128]{1,0:T(8,128)(2,1)S(1)} %collective-permute-done.2), channel_id=1, source_target_pairs={{0,8},{8,16},{16,24},{24,32},{32,40},{40,48},{48,56},{56,64},{64,7... | collective-permute-start | bytes 540680 | tf_op jit(solution)/shard_map/ppermute | solution.py:16
  168.8 9.4 %collective-permute-start.5 = (bf16[704,128]{1,0:T(8,128)(2,1)S(1)}, bf16[704,128]{1,0:T(8,128)(2,1)S(1)}, u32[]{:S(2)}, u32[]{:S(2)}) collective-permute-start(bf16[704,128]{1,0:T(8,128)(2,1)S(1)} %collective-permute-done.3), channel_id=1, source_target_pairs={{0,120},{8,0},{16,8},{24,16},{32,24},{40,32},{48,40},{56,48},{64,5... | collective-permute-start | bytes 540680 | tf_op jit(solution)/shard_map/ppermute | solution.py:21
  175.5 8.6 %collective-permute-start.6 = (bf16[704,128]{1,0:T(8,128)(2,1)S(1)}, bf16[704,128]{1,0:T(8,128)(2,1)S(1)}, u32[]{:S(2)}, u32[]{:S(2)}) collective-permute-start(bf16[704,128]{1,0:T(8,128)(2,1)S(1)} %collective-permute-done.4), channel_id=1, source_target_pairs={{0,8},{8,16},{16,24},{24,32},{32,40},{40,48},{48,56},{56,64},{64,7... | collective-permute-start | bytes 540680 | tf_op jit(solution)/shard_map/ppermute | solution.py:16
  178.3 9.5 %collective-permute-start.7 = (bf16[704,128]{1,0:T(8,128)(2,1)S(1)}, bf16[704,128]{1,0:T(8,128)(2,1)S(1)}, u32[]{:S(2)}, u32[]{:S(2)}) collective-permute-start(bf16[704,128]{1,0:T(8,128)(2,1)S(1)} %collective-permute-done.5), channel_id=1, source_target_pairs={{0,120},{8,0},{16,8},{24,16},{32,24},{40,32},{48,40},{56,48},{64,5... | collective-permute-start | bytes 540680 | tf_op jit(solution)/shard_map/ppermute | solution.py:21
  184.1 7.4 %collective-permute-start.8 = (bf16[704,128]{1,0:T(8,128)(2,1)S(1)}, bf16[704,128]{1,0:T(8,128)(2,1)S(1)}, u32[]{:S(2)}, u32[]{:S(2)}) collective-permute-start(bf16[704,128]{1,0:T(8,128)(2,1)S(1)} %collective-permute-done.6), channel_id=1, source_target_pairs={{0,8},{8,16},{16,24},{24,32},{32,40},{40,48},{48,56},{56,64},{64,7... | collective-permute-start | bytes 540680 | tf_op jit(solution)/shard_map/ppermute | solution.py:16
  187.8 9.3 %collective-permute-start.9 = (bf16[704,128]{1,0:T(8,128)(2,1)S(1)}, bf16[704,128]{1,0:T(8,128)(2,1)S(1)}, u32[]{:S(2)}, u32[]{:S(2)}) collective-permute-start(bf16[704,128]{1,0:T(8,128)(2,1)S(1)} %collective-permute-done.7), channel_id=1, source_target_pairs={{0,120},{8,0},{16,8},{24,16},{32,24},{40,32},{48,40},{56,48},{64,5... | collective-permute-start | bytes 540680 | tf_op jit(solution)/shard_map/ppermute | solution.py:21
  191.5 9.0 %collective-permute-start.10 = (bf16[704,128]{1,0:T(8,128)(2,1)S(1)}, bf16[704,128]{1,0:T(8,128)(2,1)S(1)}, u32[]{:S(2)}, u32[]{:S(2)}) collective-permute-start(bf16[704,128]{1,0:T(8,128)(2,1)S(1)} %collective-permute-done.8), channel_id=1, source_target_pairs={{0,8},{8,16},{16,24},{24,32},{32,40},{40,48},{48,56},{56,64},{64,7... | collective-permute-start | bytes 540680 | tf_op jit(solution)/shard_map/ppermute | solution.py:16
  197.1 7.2 %collective-permute-start.11 = (bf16[704,128]{1,0:T(8,128)(2,1)S(1)}, bf16[704,128]{1,0:T(8,128)(2,1)S(1)}, u32[]{:S(2)}, u32[]{:S(2)}) collective-permute-start(bf16[704,128]{1,0:T(8,128)(2,1)S(1)} %collective-permute-done.9), channel_id=1, source_target_pairs={{0,120},{8,0},{16,8},{24,16},{32,24},{40,32},{48,40},{56,48},{64,5... | collective-permute-start | bytes 540680 | tf_op jit(solution)/shard_map/ppermute | solution.py:21
  200.5 10.0 %collective-permute-start.12 = (bf16[704,128]{1,0:T(8,128)(2,1)S(1)}, bf16[704,128]{1,0:T(8,128)(2,1)S(1)}, u32[]{:S(2)}, u32[]{:S(2)}) collective-permute-start(bf16[704,128]{1,0:T(8,128)(2,1)S(1)} %collective-permute-done.10), channel_id=1, source_target_pairs={{0,8},{8,16},{16,24},{24,32},{32,40},{40,48},{48,56},{56,64},{64,7... | collective-permute-start | bytes 540680 | tf_op jit(solution)/shard_map/ppermute | solution.py:16
  204.3 7.8 %collective-permute-start.13 = (bf16[704,128]{1,0:T(8,128)(2,1)S(1)}, bf16[704,128]{1,0:T(8,128)(2,1)S(1)}, u32[]{:S(2)}, u32[]{:S(2)}) collective-permute-start(bf16[704,128]{1,0:T(8,128)(2,1)S(1)} %collective-permute-done.11), channel_id=1, source_target_pairs={{0,120},{8,0},{16,8},{24,16},{32,24},{40,32},{48,40},{56,48},{64,5... | collective-permute-start | bytes 540680 | tf_op jit(solution)/shard_map/ppermute | solution.py:21
  210.5 8.8 %collective-permute-start.14 = (bf16[704,128]{1,0:T(8,128)(2,1)S(1)}, bf16[704,128]{1,0:T(8,128)(2,1)S(1)}, u32[]{:S(2)}, u32[]{:S(2)}) collective-permute-start(bf16[704,128]{1,0:T(8,128)(2,1)S(1)} %collective-permute-done.12), channel_id=1, source_target_pairs={{0,8},{8,16},{16,24},{24,32},{32,40},{40,48},{48,56},{56,64},{64,7... | collective-permute-start | bytes 540680 | tf_op jit(solution)/shard_map/ppermute | solution.py:16
  223.0 4.5 %copy-start.6 = (f32[2048]{0:T(1024)S(1)}, f32[2048]{0:T(1024)}, u32[]{:S(2)}) copy-start(f32[2048]{0:T(1024)} %param.19) | copy-start | bytes 24580
  241.5 50.1 %copy-start.1 = (f32[3,1024]{1,0:T(4,128)S(1)}, f32[3,1024]{1,0:T(4,128)}, u32[]{:S(2)}) copy-start(f32[3,1024]{1,0:T(4,128)} %param.17) | copy-start | bytes 36868
  281.7 9.0 %all-to-all-start.5 = ((f32[8,1,512]{2,1,0:T(1,128)}), f32[8,1,512]{2,1,0:T(1,128)S(1)}, u32[]{:S(2)}, u32[]{:S(2)}) async-start(f32[8,1,512]{2,1,0:T(1,128)} %broadcast_in_dim.28), calls=%async_computation.5 | async-start | bytes 32768 | tf_op jit(solution)/shard_map/all_to_all | solution.py:36
Sparse Core Ops, SparseCore 0:
  9.1 88.9 all-gather.2
  99.9 121.5 all-gather.4
